TPU v7x, 512 devices: a whole 4x4x16 slice. The times are simulated.
512 devices in a mesh: dp: 4 (over x), kv: 64 (over z, y), tp: 2 (over core).
Axes of the slice: x: 4, y: 4, z: 16, core: 2. Of those that a mesh axis runs over, the one named last changes fastest.
Arguments:
- tokens: bfloat16 [4, 20480, 2048], P('dp', 'kv'), may hold values from -72 to 72
- w_query: bfloat16 [2048, 512], P(None, 'tp'), may hold values from -0.125 to 0.125
- key_weight: bfloat16 [2048, 256], P(None, 'tp'), may hold values from -0.125 to 0.125
- value_weight: bfloat16 [2048, 256], P(None, 'tp'), may hold values from -2.09375 to 2.09375
- w_out: bfloat16 [512, 2048], P(None, 'tp'), may hold values from -0.25 to 0.25
- chosen: int32 [4, 640, 16], P('dp', 'kv'), may hold values from -1 to 639, as said below
Outputs:
- mixed: bfloat16 [4, 20480, 2048], P('dp', 'kv', 'tp')
- log_mass: float32 [4, 4, 20480], P('dp', 'tp', 'kv')
Inputs may be any that keep to these rules, and one draw needn't show every extreme that they name: `chosen`: entry 0 of row i of a sequence is i; the other entries are distinct blocks before i, or -1 for an empty slot. The 10 rows of one index of kv together name at most one block held by any other index of kv; this bound is reached.
All inputs are finite; a program needn't handle non-finite values.
Results may differ from a plain program's by a relative error of at most 0.006.
The roundings to bfloat16 on the way count: a program that leaves them out, or rounds other values in their place, can miss the bound.
Values may be sent and summed in bfloat16 or wider, within the bound.
A program may use at most 64 MiB of HBM per device.

v0:
```python
import jax
import jax.numpy as jnp
from jax import lax
from jax.sharding import PartitionSpec as P

HEAD_WIDTH = 128


def body(tokens, w_query, key_weight, value_weight, w_out, chosen):
    local_tokens = tokens[0]
    local_chosen = chosen[0]
    row_count = local_tokens.shape[0]
    blocks_here, select_count = local_chosen.shape
    block_rows = row_count // blocks_here
    kv_heads = key_weight.shape[1] // HEAD_WIDTH
    query_heads = w_query.shape[1] // HEAD_WIDTH
    heads_per_group = query_heads // kv_heads
    width_kv = kv_heads * HEAD_WIDTH
    devices = lax.axis_size("kv")
    my_index = lax.axis_index("kv")
    queries = jnp.dot(local_tokens, w_query, preferred_element_type=jnp.float32).astype(
        jnp.bfloat16
    )
    projected_keys = jnp.dot(local_tokens, key_weight, preferred_element_type=jnp.float32).astype(
        jnp.bfloat16
    )
    projected_values = jnp.dot(
        local_tokens, value_weight, preferred_element_type=jnp.float32
    ).astype(jnp.bfloat16)
    paired = jnp.concatenate([projected_keys, projected_values], axis=1)
    owners = local_chosen // blocks_here
    inner_ix = local_chosen % blocks_here
    remote = (local_chosen >= 0) & (owners != my_index)
    peer_ids = jnp.arange(devices, dtype=jnp.int32)
    requests = jnp.where(
        remote[..., None] & (owners[..., None] == peer_ids), inner_ix[..., None], -1
    )
    wanted = jnp.max(requests, axis=(0, 1)).reshape(devices, 1)
    asked_ids = lax.all_to_all(wanted, "kv", split_axis=0, concat_axis=0, tiled=True)
    own_blocks = paired.reshape(blocks_here, block_rows, 2 * width_kv)
    replies = jnp.take(own_blocks, jnp.maximum(asked_ids[:, 0], 0), axis=0)
    arrived = lax.all_to_all(replies, "kv", split_axis=0, concat_axis=0, tiled=True)
    block_table = jnp.concatenate([arrived, own_blocks], axis=0)
    lookup = jnp.where(remote, owners, devices + inner_ix)
    picked = jnp.take(block_table, lookup, axis=0)
    selected_keys = picked[..., :width_kv].reshape(
        blocks_here, select_count * block_rows, kv_heads, HEAD_WIDTH
    )
    selected_values = picked[..., width_kv:].reshape(
        blocks_here, select_count * block_rows, kv_heads, HEAD_WIDTH
    )
    grouped_queries = queries.reshape(
        blocks_here, block_rows, kv_heads, heads_per_group, HEAD_WIDTH
    )
    scores = jnp.einsum(
        "btkgd,bskd->bkgts", grouped_queries, selected_keys, preferred_element_type=jnp.float32
    ) * HEAD_WIDTH ** (-0.5)
    bounded_index = jnp.maximum(local_chosen, 0)
    key_pos = (
        bounded_index[..., None] * block_rows + jnp.arange(block_rows, dtype=jnp.int32)
    ).reshape(blocks_here, select_count * block_rows)
    key_live = jnp.repeat(local_chosen >= 0, block_rows, axis=1)
    block_ids = my_index * blocks_here + jnp.arange(blocks_here, dtype=jnp.int32)
    query_pos = block_ids[:, None] * block_rows + jnp.arange(block_rows, dtype=jnp.int32)[None, :]
    allowed = key_live[:, None, :] & (key_pos[:, None, :] <= query_pos[:, :, None])
    scores = jnp.where(allowed[:, None, None], scores, -jnp.inf)
    row_max = jnp.max(scores, axis=-1)
    weights = jnp.exp(scores - row_max[..., None])
    row_sum = jnp.sum(weights, axis=-1)
    probs_low = weights.astype(jnp.bfloat16)
    summed = jnp.einsum(
        "bkgts,bskd->btkgd", probs_low, selected_values, preferred_element_type=jnp.float32
    )
    attended = (
        (summed / row_sum.transpose(0, 3, 1, 2)[..., None])
        .astype(jnp.bfloat16)
        .reshape(row_count, query_heads * HEAD_WIDTH)
    )
    log_mass = (row_max + jnp.log(row_sum)).transpose(1, 2, 0, 3).reshape(query_heads, row_count)
    mixed = jnp.dot(
        lax.all_gather(attended, "tp", axis=1, tiled=True),
        w_out,
        preferred_element_type=jnp.float32,
    ).astype(jnp.bfloat16)
    return (mixed[None], log_mass[None])


def solution(mesh):
    in_specs = (
        P("dp", "kv", None),
        P(None, "tp"),
        P(None, "tp"),
        P(None, "tp"),
        P(None, "tp"),
        P("dp", "kv", None),
    )
    out_specs = (P("dp", "kv", "tp"), P("dp", "tp", "kv"))
    return jax.shard_map(body, mesh=mesh, in_specs=in_specs, out_specs=out_specs, check_vma=False)
```

profile of v0, /device:TPU:1, one launch (start us, length us, event | category | flops | bytes accessed | tf_op | source)
XLA Modules:
  0.0 116.2 jit_solution(6678006061197199242)
XLA Ops:
  0.6 0.0 copy-start
  0.6 0.0 copy-start.2
  0.7 0.8 broadcast_remainder_fusion
  1.5 0.7 compare_and_fusion.1
  2.2 0.1 select_reduce_fusion
  2.4 0.7 copy.58
  3.1 19.3 %all-to-all-start = ((s32[64,1,1]{2,1,0:T(1,128)}), s32[64,1,1]{2,1,0:T(1,128)S(1)}, u32[]{:S(2)}, u32[]{:S(2)}) async-start(s32[64,1,1]{2,1,0:T(1,128)} %copy.58), calls=%async_computation | async-start | bytes 65536 | tf_op jit(solution)/shard_map/all_to_all | solution.py:39
  22.4 0.0 copy-done
  22.4 1.5 %fusion.14 = bf16[320,128]{1,0:T(8,128)(2,1)S(1)} fusion(bf16[2048,128]{1,0:T(8,128)(2,1)} %param.8, bf16[1,320,2048]{2,1,0:T(8,128)(2,1)S(1)} %copy-done), kind=kOutput, calls=%fused_computation.20 | convolution fusion | flops 167813120 | bytes 1916928 | tf_op jit(solution)/shard_map/dot_general | solution.py:24
  23.9 0.0 copy-done.2
  23.9 0.5 fusion.17
  24.5 11.3 %all-to-all-done = s32[64,1,1]{2,1,0:T(1,128)S(1)} async-done(((s32[64,1,1]{2,1,0:T(1,128)}), s32[64,1,1]{2,1,0:T(1,128)S(1)}, u32[]{:S(2)}, u32[]{:S(2)}) %all-to-all-start) | async-done | bytes 288 | tf_op jit(solution)/shard_map/all_to_all | solution.py:39
  35.8 1.2 %maximum_reduce_fusion = s32[64]{0:T(128)S(1)} fusion(s32[64,1,1]{2,1,0:T(1,128)S(1)} %all-to-all-done), kind=kLoop, calls=%fused_computation.41 | loop fusion | flops 64 | bytes 512 | tf_op jit(solution)/shard_map/max | solution.py:41
  37.0 0.6 gather_fusion
  37.6 1.2 %compare_reduce_fusion = pred[64]{0:T(512)(128)(4,1)S(1)} fusion(s32[64,1,1]{2,1,0:T(1,128)S(1)} %all-to-all-done), kind=kLoop, calls=%fused_computation.31 | loop fusion | flops 128 | bytes 320 | tf_op jit(solution)/shard_map/jit(_take)/le | solution.py:41
  38.9 1.2 %broadcast_select_fusion.1 = bf16[64,32,256]{2,1,0:T(8,128)(2,1)} fusion(bf16[64,32,256]{2,1,0:T(8,128)(2,1)S(1)} %gather_fusion, pred[64]{0:T(512)(128)(4,1)S(1)} %compare_reduce_fusion), kind=kLoop, calls=%fused_computation.24 | loop fusion | flops 524288 | bytes 2097216 | tf_op jit(solution)/shard_map/jit(_take)/select_n | solution.py:41
  40.1 0.0 copy-start.3
  40.1 0.0 copy-start.4
  40.1 5.6 %all-to-all-start.1 = ((bf16[64,32,256]{2,1,0:T(8,128)(2,1)}), bf16[64,32,256]{2,1,0:T(8,128)(2,1)}, u32[]{:S(2)}, u32[]{:S(2)}) async-start(bf16[64,32,256]{2,1,0:T(8,128)(2,1)} %broadcast_select_fusion.1), calls=%async_computation.1 | async-start | bytes 2097152 | tf_op jit(solution)/shard_map/all_to_all | solution.py:42
  45.7 0.0 copy-done.3
  45.8 0.1 fusion.33
  45.9 0.1 reshape.281
  45.9 0.1 broadcast_in_dim.68
  46.0 0.1 and.100
  46.1 0.1 add.151
  46.2 0.1 add.152
  46.3 0.1 add.154
  46.4 0.0 copy-done.4
  46.4 0.5 fusion.9
  47.0 0.1 iota_add_fusion
  47.1 0.2 compare_and_fusion
  47.3 49.6 %all-to-all-done.1 = bf16[64,32,256]{2,1,0:T(8,128)(2,1)} async-done(((bf16[64,32,256]{2,1,0:T(8,128)(2,1)}), bf16[64,32,256]{2,1,0:T(8,128)(2,1)}, u32[]{:S(2)}, u32[]{:S(2)}) %all-to-all-start.1) | async-done | bytes 1048608 | tf_op jit(solution)/shard_map/all_to_all | solution.py:42
  96.9 1.3 %pad_maximum_fusion = bf16[74,32,256]{2,1,0:T(8,128)(2,1)S(1)} fusion(bf16[10,32,256]{2,1,0:T(8,128)(2,1)S(1)} %bitcast.114, bf16[64,32,256]{2,1,0:T(8,128)(2,1)} %all-to-all-done.1), kind=kLoop, calls=%fused_computation.15 | loop fusion | flops 606208 | bytes 2424832 | tf_op jit(solution)/shard_map/concatenate | solution.py:43
  98.3 2.5 %gather_fusion.1 = bf16[160,32,256]{2,1,0:T(8,128)(2,1)} fusion(bf16[74,32,256]{2,1,0:T(8,128)(2,1)S(1)} %pad_maximum_fusion, s32[1024]{0:T(1024)S(1)} %pad_clamp_fusion), kind=kCustom, calls=%fused_computation.1 | custom fusion | bytes 5243520 | tf_op jit(solution)/shard_map/jit(_take)/gather | solution.py:45
  100.8 2.1 %broadcast_select_fusion = bf16[10,16,32,256]{3,2,1,0:T(8,128)(2,1)S(1)} fusion(bf16[10,16,32,256]{3,2,1,0:T(8,128)(2,1)} %bitcast.115, pred[10,16]{1,0:T(8,128)(4,1)S(1)} %get-tuple-element.2), kind=kLoop, calls=%fused_computation.2 | loop fusion | flops 1310720 | bytes 5243040 | tf_op jit(solution)/shard_map/jit(_take)/select_n | solution.py:45
  102.8 1.5 %fusion.37 = (bf16[10,16,32,128]{3,2,1,0:T(8,128)(2,1)S(1)}, bf16[10,16,32,128]{3,2,1,0:T(8,128)(2,1)}) fusion(bf16[10,16,32,256]{3,2,1,0:T(8,128)(2,1)S(1)} %broadcast_select_fusion), kind=kLoop, calls=%fused_computation.71 | loop fusion | bytes 5242880 | tf_op jit(solution)/shard_map/slice | solution.py:46
  104.3 0.7 fusion.38
  105.0 0.5 fusion.12
  105.5 0.7 broadcast_in_dim_reshape.2
  106.2 1.8 %fusion.21 = bf16[10,32,1,2,128]{4,1,3,0,2:T(8,128)(2,1)S(1)} fusion(bf16[10,512,128,1]{2,1,3,0:T(8,128)(2,1)} %bitcast.117, f32[10,1,2,32,512]{4,3,2,0,1:T(8,128)S(1)} %get-tuple-element.11, f32[10,2,32]{2,1,0:T(2,128)S(1)} %get-tuple-element.10, f32[10,32,2]{1,2,0:T(2,128)S(1)} %bitcast.120), kind=kOutput, calls=%fused_computation.23 | convolution fusion | flops 84705280 | bytes 2790400 | tf_op jit(solution)/shard_map/bkgts,bskd->btkgd/dot_general | solution.py:71
  107.9 0.0 copy-start.1
  107.9 0.1 copy.64
  108.1 6.7 %all_gather.3 = bf16[320,512]{1,0:T(8,128)(2,1)S(1)} all-gather(bf16[320,256]{1,0:T(8,128)(2,1)S(1)} %bitcast.119), channel_id=1, replica_groups=mesh['dp'=4,'kv'=64,'tp'=2] {'tp'}, dimensions={1}, use_global_device_ids=true | all-gather | bytes 491520 | tf_op jit(solution)/shard_map/all_gather | solution.py:81
  114.8 0.0 copy-done.1
  114.8 1.3 %fusion.8 = bf16[1,320,1024]{2,1,0:T(8,128)(2,1)} fusion(bf16[320,512]{1,0:T(8,128)(2,1)S(1)} %all_gather.3, bf16[512,1024]{1,0:T(8,128)(2,1)S(1)} %copy-done.1), kind=kOutput, calls=%fused_computation.14 | convolution fusion | flops 335872000 | bytes 2031616 | tf_op jit(solution)/shard_map/dot_general | solution.py:80
  (14 shorter events, 0.2 us)
Async XLA Ops:
  0.6 21.7 %copy-start = (bf16[1,320,2048]{2,1,0:T(8,128)(2,1)S(1)}, bf16[1,320,2048]{2,1,0:T(8,128)(2,1)}, u32[]{:S(2)}) copy-start(bf16[1,320,2048]{2,1,0:T(8,128)(2,1)} %param.6) | copy-start | bytes 3932164
  0.6 23.3 %copy-start.2 = (bf16[2048,128]{1,0:T(8,128)(2,1)S(1)}, bf16[2048,128]{1,0:T(8,128)(2,1)}, u32[]{:S(2)}) copy-start(bf16[2048,128]{1,0:T(8,128)(2,1)} %param.9) | copy-start | bytes 1572868
  3.1 32.7 %all-to-all-start = ((s32[64,1,1]{2,1,0:T(1,128)}), s32[64,1,1]{2,1,0:T(1,128)S(1)}, u32[]{:S(2)}, u32[]{:S(2)}) async-start(s32[64,1,1]{2,1,0:T(1,128)} %copy.58), calls=%async_computation | async-start | bytes 65536 | tf_op jit(solution)/shard_map/all_to_all | solution.py:39
  40.1 5.7 %copy-start.3 = (s32[1,10,16]{2,0,1:T(1,128)S(1)}, s32[1,10,16]{2,0,1:T(1,128)}, u32[]{:S(2)}) copy-start(s32[1,10,16]{2,0,1:T(1,128)} %param.11) | copy-start | bytes 1924
  40.1 6.3 %copy-start.4 = (bf16[2048,256]{1,0:T(8,128)(2,1)S(1)}, bf16[2048,256]{1,0:T(8,128)(2,1)}, u32[]{:S(2)}) copy-start(bf16[2048,256]{1,0:T(8,128)(2,1)} %param.7) | copy-start | bytes 3145732
  40.1 56.9 %all-to-all-start.1 = ((bf16[64,32,256]{2,1,0:T(8,128)(2,1)}), bf16[64,32,256]{2,1,0:T(8,128)(2,1)}, u32[]{:S(2)}, u32[]{:S(2)}) async-start(bf16[64,32,256]{2,1,0:T(8,128)(2,1)} %broadcast_select_fusion.1), calls=%async_computation.1 | async-start | bytes 2097152 | tf_op jit(solution)/shard_map/all_to_all | solution.py:42
  107.9 6.9 %copy-start.1 = (bf16[512,1024]{1,0:T(8,128)(2,1)S(1)}, bf16[512,1024]{1,0:T(8,128)(2,1)}, u32[]{:S(2)}) copy-start(bf16[512,1024]{1,0:T(8,128)(2,1)} %param.10) | copy-start | bytes 3145732
where the time goes:
time: 117 us; the launch traced here: 116 us
  waiting for transfers between devices  60.9 us (52%)
  starting transfers between devices  24.9 us (21%)
  other arithmetic  9.62 us (8%)
  local copies, waits for them, and re-layouts  6.76 us (6%)
  blocking collectives  6.68 us (6%)
  matrix products  6.38 us (5%)
    all_to_all x1, waiting for transfers between devices, body(): lax.all_to_all(replies, 'kv', split_axis=0, concat_axis=0, tiled=True)  49.6 us
    all_to_all x1, starting transfers between devices, body(): lax.all_to_all(wanted, 'kv', split_axis=0, concat_axis=0, tiled=True)  19.3 us
    all_to_all x1, waiting for transfers between devices, body(): lax.all_to_all(wanted, 'kv', split_axis=0, concat_axis=0, tiled=True)  11.3 us
    all_gather x1, blocking collectives, body(): lax.all_gather(attended, 'tp', axis=1, tiled=True)  6.68 us
    all_to_all x1, starting transfers between devices, body(): lax.all_to_all(replies, 'kv', split_axis=0, concat_axis=0, tiled=True)  5.64 us
    gather x1, local copies, waits for them, and re-layouts, body(): picked = jnp.take(block_table, lookup, axis=0)  2.48 us
  transfers between devices with their start and end apart: 2, of which 2 were waited for; matrix products, arithmetic and copies ran while one was open for 3% of the time, Pallas kernels for 0%

commit v1 on v0

--- a/solution.py
+++ b/solution.py
@@ -4,6 +4,12 @@
 from jax.sharding import PartitionSpec as P
 
 HEAD_WIDTH = 128
+
+
+def gather_by_exchange(x, axis, dim):
+    count = lax.axis_size(axis)
+    repeats = [count if d == dim else 1 for d in range(x.ndim)]
+    return lax.all_to_all(jnp.tile(x, repeats), axis, split_axis=dim, concat_axis=dim, tiled=True)
 
 
 def body(tokens, w_query, key_weight, value_weight, w_out, chosen):
@@ -78,9 +84,7 @@
     )
     log_mass = (row_max + jnp.log(row_sum)).transpose(1, 2, 0, 3).reshape(query_heads, row_count)
     mixed = jnp.dot(
-        lax.all_gather(attended, "tp", axis=1, tiled=True),
-        w_out,
-        preferred_element_type=jnp.float32,
+        gather_by_exchange(attended, "tp", 1), w_out, preferred_element_type=jnp.float32
     ).astype(jnp.bfloat16)
     return (mixed[None], log_mass[None])
 

time: 117 us -> 119 us (1.017)
  blocking collectives: 6.68 us -> 8.64 us
    all_to_all x0 -> x1, blocking collectives: none -> 8.64 us  [gather_by_exchange(): lax.all_to_all(jnp.tile(x, repeats), axis, split_axis=dim, concat_axis=di...]
    all_gather x1 -> x0, blocking collectives: 6.68 us -> none  [body(): lax.all_gather(attended, 'tp', axis=1, tiled=True)]
where the time goes in v1:
time: 119 us; the launch traced here: 118 us
  waiting for transfers between devices  60.9 us (51%)
  starting transfers between devices  24.9 us (21%)
  other arithmetic  9.62 us (8%)
  blocking collectives  8.64 us (7%)
  local copies, waits for them, and re-layouts  6.8 us (6%)
  matrix products  6.38 us (5%)
    all_to_all x1, waiting for transfers between devices, body(): lax.all_to_all(replies, 'kv', split_axis=0, concat_axis=0, tiled=True)  49.6 us
    all_to_all x1, starting transfers between devices, body(): lax.all_to_all(wanted, 'kv', split_axis=0, concat_axis=0, tiled=True)  19.3 us
    all_to_all x1, waiting for transfers between devices, body(): lax.all_to_all(wanted, 'kv', split_axis=0, concat_axis=0, tiled=True)  11.3 us
    all_to_all x1, blocking collectives, gather_by_exchange(): lax.all_to_all(jnp.tile(x, repeats), axis, split_axis=dim, concat_axis=di...  8.64 us
    all_to_all x1, starting transfers between devices, body(): lax.all_to_all(replies, 'kv', split_axis=0, concat_axis=0, tiled=True)  5.64 us
    gather x1, local copies, waits for them, and re-layouts, body(): picked = jnp.take(block_table, lookup, axis=0)  2.48 us
  transfers between devices with their start and end apart: 2, of which 2 were waited for; matrix products, arithmetic and copies ran while one was open for 3% of the time, Pallas kernels for 0%

profile of v1, /device:TPU:1, one launch (start us, length us, event | category | flops | bytes accessed | tf_op | source)
XLA Modules:
  0.0 118.2 jit_solution(7122992352431941331)
XLA Ops:
  0.6 0.0 copy-start
  0.6 0.0 copy-start.2
  0.7 0.8 broadcast_remainder_fusion
  1.5 0.7 compare_and_fusion.1
  2.2 0.1 select_reduce_fusion
  2.4 0.7 copy.59
  3.1 19.3 %all-to-all-start = ((s32[64,1,1]{2,1,0:T(1,128)}), s32[64,1,1]{2,1,0:T(1,128)S(1)}, u32[]{:S(2)}, u32[]{:S(2)}) async-start(s32[64,1,1]{2,1,0:T(1,128)} %copy.59), calls=%async_computation | async-start | bytes 65536 | tf_op jit(solution)/shard_map/all_to_all | solution.py:45
  22.4 0.0 copy-done
  22.4 1.5 %fusion.14 = bf16[320,128]{1,0:T(8,128)(2,1)S(1)} fusion(bf16[2048,128]{1,0:T(8,128)(2,1)} %param.8, bf16[1,320,2048]{2,1,0:T(8,128)(2,1)S(1)} %copy-done), kind=kOutput, calls=%fused_computation.20 | convolution fusion | flops 167813120 | bytes 1916928 | tf_op jit(solution)/shard_map/dot_general | solution.py:30
  23.9 0.0 copy-done.2
  23.9 0.5 fusion.17
  24.5 11.3 %all-to-all-done = s32[64,1,1]{2,1,0:T(1,128)S(1)} async-done(((s32[64,1,1]{2,1,0:T(1,128)}), s32[64,1,1]{2,1,0:T(1,128)S(1)}, u32[]{:S(2)}, u32[]{:S(2)}) %all-to-all-start) | async-done | bytes 288 | tf_op jit(solution)/shard_map/all_to_all | solution.py:45
  35.8 1.2 %maximum_reduce_fusion = s32[64]{0:T(128)S(1)} fusion(s32[64,1,1]{2,1,0:T(1,128)S(1)} %all-to-all-done), kind=kLoop, calls=%fused_computation.41 | loop fusion | flops 64 | bytes 512 | tf_op jit(solution)/shard_map/max | solution.py:47
  37.0 0.6 gather_fusion
  37.6 1.2 %compare_reduce_fusion = pred[64]{0:T(512)(128)(4,1)S(1)} fusion(s32[64,1,1]{2,1,0:T(1,128)S(1)} %all-to-all-done), kind=kLoop, calls=%fused_computation.31 | loop fusion | flops 128 | bytes 320 | tf_op jit(solution)/shard_map/jit(_take)/le | solution.py:47
  38.9 1.2 %broadcast_select_fusion.1 = bf16[64,32,256]{2,1,0:T(8,128)(2,1)} fusion(bf16[64,32,256]{2,1,0:T(8,128)(2,1)S(1)} %gather_fusion, pred[64]{0:T(512)(128)(4,1)S(1)} %compare_reduce_fusion), kind=kLoop, calls=%fused_computation.24 | loop fusion | flops 524288 | bytes 2097216 | tf_op jit(solution)/shard_map/jit(_take)/select_n | solution.py:47
  40.1 0.0 copy-start.3
  40.1 0.0 copy-start.4
  40.1 5.6 %all-to-all-start.1 = ((bf16[64,32,256]{2,1,0:T(8,128)(2,1)}), bf16[64,32,256]{2,1,0:T(8,128)(2,1)}, u32[]{:S(2)}, u32[]{:S(2)}) async-start(bf16[64,32,256]{2,1,0:T(8,128)(2,1)} %broadcast_select_fusion.1), calls=%async_computation.1 | async-start | bytes 2097152 | tf_op jit(solution)/shard_map/all_to_all | solution.py:48
  45.7 0.0 copy-done.3
  45.8 0.1 fusion.33
  45.9 0.1 reshape.284
  45.9 0.1 broadcast_in_dim.68
  46.0 0.1 and.100
  46.1 0.1 add.151
  46.2 0.1 add.152
  46.3 0.1 add.154
  46.4 0.0 copy-done.4
  46.4 0.5 fusion.9
  47.0 0.1 iota_add_fusion
  47.1 0.2 compare_and_fusion
  47.3 49.6 %all-to-all-done.1 = bf16[64,32,256]{2,1,0:T(8,128)(2,1)} async-done(((bf16[64,32,256]{2,1,0:T(8,128)(2,1)}), bf16[64,32,256]{2,1,0:T(8,128)(2,1)}, u32[]{:S(2)}, u32[]{:S(2)}) %all-to-all-start.1) | async-done | bytes 1048608 | tf_op jit(solution)/shard_map/all_to_all | solution.py:48
  96.9 1.3 %pad_maximum_fusion = bf16[74,32,256]{2,1,0:T(8,128)(2,1)S(1)} fusion(bf16[10,32,256]{2,1,0:T(8,128)(2,1)S(1)} %bitcast.116, bf16[64,32,256]{2,1,0:T(8,128)(2,1)} %all-to-all-done.1), kind=kLoop, calls=%fused_computation.15 | loop fusion | flops 606208 | bytes 2424832 | tf_op jit(solution)/shard_map/concatenate | solution.py:49
  98.3 2.5 %gather_fusion.1 = bf16[160,32,256]{2,1,0:T(8,128)(2,1)} fusion(bf16[74,32,256]{2,1,0:T(8,128)(2,1)S(1)} %pad_maximum_fusion, s32[1024]{0:T(1024)S(1)} %pad_clamp_fusion), kind=kCustom, calls=%fused_computation.1 | custom fusion | bytes 5243520 | tf_op jit(solution)/shard_map/jit(_take)/gather | solution.py:51
  100.8 2.1 %broadcast_select_fusion = bf16[10,16,32,256]{3,2,1,0:T(8,128)(2,1)S(1)} fusion(bf16[10,16,32,256]{3,2,1,0:T(8,128)(2,1)} %bitcast.117, pred[10,16]{1,0:T(8,128)(4,1)S(1)} %get-tuple-element.2), kind=kLoop, calls=%fused_computation.2 | loop fusion | flops 1310720 | bytes 5243040 | tf_op jit(solution)/shard_map/jit(_take)/select_n | solution.py:51
  102.8 1.5 %fusion.37 = (bf16[10,16,32,128]{3,2,1,0:T(8,128)(2,1)S(1)}, bf16[10,16,32,128]{3,2,1,0:T(8,128)(2,1)}) fusion(bf16[10,16,32,256]{3,2,1,0:T(8,128)(2,1)S(1)} %broadcast_select_fusion), kind=kLoop, calls=%fused_computation.71 | loop fusion | bytes 5242880 | tf_op jit(solution)/shard_map/slice | solution.py:52
  104.3 0.7 fusion.38
  105.0 0.5 fusion.12
  105.5 0.7 broadcast_in_dim_reshape.2
  106.2 1.8 %fusion.21 = bf16[10,32,1,2,128]{4,1,3,0,2:T(8,128)(2,1)S(1)} fusion(bf16[10,512,128,1]{2,1,3,0:T(8,128)(2,1)} %bitcast.119, f32[10,1,2,32,512]{4,3,2,0,1:T(8,128)S(1)} %get-tuple-element.11, f32[10,2,32]{2,1,0:T(2,128)S(1)} %get-tuple-element.10, f32[10,32,2]{1,2,0:T(2,128)S(1)} %bitcast.124), kind=kOutput, calls=%fused_computation.23 | convolution fusion | flops 84705280 | bytes 2790400 | tf_op jit(solution)/shard_map/bkgts,bskd->btkgd/dot_general | solution.py:77
  107.9 0.0 copy-start.1
  107.9 0.1 copy.65
  108.2 8.6 %all_to_all.23 = bf16[320,2,256]{2,0,1:T(8,128)(2,1)S(1)} all-to-all(bf16[320,2,256]{2,0,1:T(8,128)(2,1)S(1)} %tile.9), channel_id=1, replica_groups=mesh['dp'=4,'kv'=64,'tp'=2] {'tp'}, dimensions={1} | all-to-all | bytes 655360 | tf_op jit(solution)/shard_map/all_to_all | solution.py:12
  116.8 0.0 copy-done.1
  116.8 1.3 %fusion.8 = bf16[1,320,1024]{2,1,0:T(8,128)(2,1)} fusion(bf16[320,512]{1,0:T(8,128)(2,1)S(1)} %bitcast.120, bf16[512,1024]{1,0:T(8,128)(2,1)S(1)} %copy-done.1), kind=kOutput, calls=%fused_computation.14 | convolution fusion | flops 335872000 | bytes 2031616 | tf_op jit(solution)/shard_map/dot_general | solution.py:86
  (16 shorter events, 0.2 us)
Async XLA Ops:
  0.6 21.7 %copy-start = (bf16[1,320,2048]{2,1,0:T(8,128)(2,1)S(1)}, bf16[1,320,2048]{2,1,0:T(8,128)(2,1)}, u32[]{:S(2)}) copy-start(bf16[1,320,2048]{2,1,0:T(8,128)(2,1)} %param.6) | copy-start | bytes 3932164
  0.6 23.3 %copy-start.2 = (bf16[2048,128]{1,0:T(8,128)(2,1)S(1)}, bf16[2048,128]{1,0:T(8,128)(2,1)}, u32[]{:S(2)}) copy-start(bf16[2048,128]{1,0:T(8,128)(2,1)} %param.9) | copy-start | bytes 1572868
  3.1 32.7 %all-to-all-start = ((s32[64,1,1]{2,1,0:T(1,128)}), s32[64,1,1]{2,1,0:T(1,128)S(1)}, u32[]{:S(2)}, u32[]{:S(2)}) async-start(s32[64,1,1]{2,1,0:T(1,128)} %copy.59), calls=%async_computation | async-start | bytes 65536 | tf_op jit(solution)/shard_map/all_to_all | solution.py:45
  40.1 5.7 %copy-start.3 = (s32[1,10,16]{2,0,1:T(1,128)S(1)}, s32[1,10,16]{2,0,1:T(1,128)}, u32[]{:S(2)}) copy-start(s32[1,10,16]{2,0,1:T(1,128)} %param.11) | copy-start | bytes 1924
  40.1 6.3 %copy-start.4 = (bf16[2048,256]{1,0:T(8,128)(2,1)S(1)}, bf16[2048,256]{1,0:T(8,128)(2,1)}, u32[]{:S(2)}) copy-start(bf16[2048,256]{1,0:T(8,128)(2,1)} %param.7) | copy-start | bytes 3145732
  40.1 56.9 %all-to-all-start.1 = ((bf16[64,32,256]{2,1,0:T(8,128)(2,1)}), bf16[64,32,256]{2,1,0:T(8,128)(2,1)}, u32[]{:S(2)}, u32[]{:S(2)}) async-start(bf16[64,32,256]{2,1,0:T(8,128)(2,1)} %broadcast_select_fusion.1), calls=%async_computation.1 | async-start | bytes 2097152 | tf_op jit(solution)/shard_map/all_to_all | solution.py:48
  107.9 8.9 %copy-start.1 = (bf16[512,1024]{1,0:T(8,128)(2,1)S(1)}, bf16[512,1024]{1,0:T(8,128)(2,1)}, u32[]{:S(2)}) copy-start(bf16[512,1024]{1,0:T(8,128)(2,1)} %param.10) | copy-start | bytes 3145732
